TPU v7x, 128 devices: a whole 4x4x4 slice. The times are simulated.
128 devices in a mesh: sp: 16 (over z, y), tp: 8 (over x, core).
Axes of the slice: x: 4, y: 4, z: 4, core: 2. Of those that a mesh axis runs over, the one named last changes fastest.
Arguments:
- residual_in: bfloat16 [16384, 2048], P(('sp', 'tp')), may hold values from -6 to 6
- queries: bfloat16 [16384, 2048], P('sp', 'tp'), may hold values from -6 to 6
- keys: bfloat16 [16384, 1024], P('sp', 'tp'), may hold values from -6 to 6
- values: bfloat16 [16384, 1024], P('sp', 'tp'), may hold values from -6 to 6
- query_gain: float32 [128], replicated, may hold values from 1 to 7
- key_norm_gain: float32 [128], replicated, may hold values from 1 to 7
- out_weight: bfloat16 [2048, 2048], replicated, may hold values from -0.125 to 0.125
- norm_gain: float32 [2048], replicated, may hold values from 0.1 to 1.9
- up_weight: bfloat16 [2048, 8192], P('sp', 'tp'), may hold values from -0.125 to 0.125
- down_weight: bfloat16 [8192, 2048], P('tp', 'sp'), may hold values from -0.0625 to 0.0625
Outputs:
- residual_out: bfloat16 [16384, 2048], P(('sp', 'tp'))
All inputs are finite; a program needn't handle non-finite values.
Results may differ from a plain program's by a relative error of at most 0.017.
The roundings to bfloat16 on the way count: a program that leaves them out, or rounds other values in their place, can miss the bound.
Values may be sent and summed in bfloat16 or wider, within the bound.
No kernel may reach another device: no remote copies, remote signals or barrier semaphores. Data moves between devices by JAX's collectives and lax.ppermute only.
A program may use at most 128 MiB of HBM per device.

v0:
```python
import jax
import jax.numpy as jnp
from jax import lax
from jax.sharding import PartitionSpec as P

HEAD_WIDTH = 128
GRID_W = 64
epsilon = 1e-06


def sent_together(arrays, axis, dim, along):
    widths = [a.shape[along] for a in arrays]
    both = jnp.concatenate(arrays, axis=along)
    filled = lax.all_gather(both, axis, axis=dim, tiled=True)
    return tuple(jnp.split(filled, [sum(widths[:k]) for k in range(1, len(widths))], axis=along))


def rope_tables(offset, count):
    places = offset + jnp.arange(count)
    grid_row = (places // GRID_W).astype(jnp.float32)
    grid_col = (places % GRID_W).astype(jnp.float32)
    quarter = HEAD_WIDTH // 4
    inverse = 10000.0 ** (-jnp.arange(quarter, dtype=jnp.float32) / quarter)
    angle_row = grid_row[:, None] * inverse
    angle_col = grid_col[:, None] * inverse
    angles = jnp.concatenate([angle_row, angle_row, angle_col, angle_col], axis=-1)
    return (jnp.cos(angles), jnp.sin(angles))


def normalize_rotate(source, gain, cosine_lookup, sine_lookup):
    count = source.shape[0]
    heads = source.shape[1] // HEAD_WIDTH
    quarter = HEAD_WIDTH // 4
    vector = source.astype(jnp.float32).reshape(count, heads, HEAD_WIDTH)
    vector = vector * lax.rsqrt(jnp.mean(vector * vector, axis=-1, keepdims=True) + epsilon) * gain
    turned = jnp.concatenate(
        [
            -vector[..., quarter : 2 * quarter],
            vector[..., :quarter],
            -vector[..., 3 * quarter :],
            vector[..., 2 * quarter : 3 * quarter],
        ],
        axis=-1,
    )
    rotated = vector * cosine_lookup[:, None, :] + turned * sine_lookup[:, None, :]
    return rotated.reshape(count, heads * HEAD_WIDTH).astype(jnp.bfloat16)


def attend(state_now, key_rows, value_rows, query_grid):
    best, mass, accum = state_now
    kv_here = query_grid.shape[1]
    key_lattice = key_rows.reshape(key_rows.shape[0], kv_here, HEAD_WIDTH)
    value_lattice = value_rows.reshape(value_rows.shape[0], kv_here, HEAD_WIDTH)
    scores = jnp.einsum(
        "tkgd,rkd->tkgr", query_grid, key_lattice, preferred_element_type=jnp.float32
    ) * HEAD_WIDTH ** (-0.5)
    newest = jnp.maximum(best, jnp.max(scores, axis=-1))
    factor = jnp.exp(best - newest)
    weights = jnp.exp(scores - newest[..., None])
    mass = mass * factor + jnp.sum(weights, axis=-1)
    accum = accum * factor[..., None] + jnp.einsum(
        "tkgr,rkd->tkgd",
        weights.astype(jnp.bfloat16),
        value_lattice,
        preferred_element_type=jnp.float32,
    )
    return (newest, mass, accum)


def local(
    residual_in,
    queries,
    keys,
    values,
    query_gain,
    key_norm_gain,
    out_weight,
    norm_gain,
    up_weight,
    down_weight,
):
    tok_rows = queries.shape[0]
    heads_here = queries.shape[1] // HEAD_WIDTH
    kv_here = keys.shape[1] // HEAD_WIDTH
    queries_per_group = heads_here // kv_here
    cosine_lookup, sine_lookup = rope_tables(lax.axis_index("sp") * tok_rows, tok_rows)
    query_normalize = normalize_rotate(queries, query_gain, cosine_lookup, sine_lookup)
    key_normalize = normalize_rotate(keys, key_norm_gain, cosine_lookup, sine_lookup)
    query_grid = query_normalize.reshape(tok_rows, kv_here, queries_per_group, HEAD_WIDTH)
    initial = (
        jnp.full((tok_rows, kv_here, queries_per_group), -1e30, jnp.float32),
        jnp.zeros((tok_rows, kv_here, queries_per_group), jnp.float32),
        jnp.zeros((tok_rows, kv_here, queries_per_group, HEAD_WIDTH), jnp.float32),
    )
    state_now = initial
    key_rows, value_rows = sent_together((key_normalize, values), "sp", 0, 1)
    row_count = key_rows.shape[0]
    key_blocks = key_rows.reshape(row_count // 1024, 1024, key_rows.shape[1])
    value_blocks = value_rows.reshape(row_count // 1024, 1024, value_rows.shape[1])

    def step_block(state_block, block_pair):
        return (attend(state_block, block_pair[0], block_pair[1], query_grid), None)

    state_now, unused = lax.scan(step_block, state_now, (key_blocks, value_blocks))
    best, mass, accum = state_now
    attn = (accum / mass[..., None]).astype(jnp.bfloat16).reshape(tok_rows, heads_here * HEAD_WIDTH)
    all_heads = lax.all_to_all(attn, "tp", split_axis=0, concat_axis=1, tiled=True)
    projected = jnp.dot(all_heads, out_weight, preferred_element_type=jnp.float32)
    middle = residual_in.astype(jnp.float32) + projected
    normed = (
        middle * lax.rsqrt(jnp.mean(middle * middle, axis=-1, keepdims=True) + epsilon) * norm_gain
    ).astype(jnp.bfloat16)
    whole_rows = lax.all_gather(normed, "tp", axis=0, tiled=True)
    hidden = jax.nn.relu(
        jnp.dot(
            whole_rows,
            lax.all_gather(up_weight, "sp", axis=0, tiled=True),
            preferred_element_type=jnp.float32,
        )
    )
    act = (hidden * hidden).astype(jnp.bfloat16)
    down_whole = lax.all_gather(down_weight, "sp", axis=1, tiled=True)
    down = lax.psum_scatter(
        jnp.dot(act, down_whole, preferred_element_type=jnp.float32).astype(jnp.bfloat16),
        "tp",
        scatter_dimension=0,
        tiled=True,
    ).astype(jnp.float32)
    return (middle + down).astype(jnp.bfloat16)


def solution(mesh):
    return jax.shard_map(
        local,
        mesh=mesh,
        in_specs=(
            P(("sp", "tp"), None),
            P("sp", "tp"),
            P("sp", "tp"),
            P("sp", "tp"),
            P(),
            P(),
            P(),
            P(),
            P("sp", "tp"),
            P("tp", "sp"),
        ),
        out_specs=P(("sp", "tp"), None),
        check_vma=False,
    )
```

profile of v0, /device:TPU:0, one launch (start us, length us, event | category | flops | bytes accessed | tf_op | source)
XLA Modules:
  0.0 411.6 jit_solution(3915185514579296366)
XLA Ops:
  6.6 1.2 fusion.26
  7.8 1.2 fusion.28
  9.0 1.6 fusion.33
  10.9 4.1 fusion.31
  17.6 1.2 copy.26
  20.4 1.2 maximum_multiply_fusion
  22.2 67.3 %all-gather.5.cloned.1.call-done = bf16[16384,256]{1,0:T(8,128)(2,1)} async-done(((bf16[1024,256]{1,0:T(8,128)(2,1)}), bf16[16384,256]{1,0:T(8,128)(2,1)}) %all-gather.5.cloned.1.call-update) | async-done | bytes 8388624 | tf_op jit(solution)/shard_map/all_gather | solution.py:14
  89.5 5.7 %fusion.46 = (bf16[16384,128]{1,0:T(8,128)(2,1)}, bf16[16384,128]{1,0:T(8,128)(2,1)}) fusion(bf16[16384,256]{1,0:T(8,128)(2,1)} %all-gather.5.cloned.1.call-done), kind=kLoop, calls=%fused_computation.85 | loop fusion | bytes 16777216 | tf_op jit(solution)/shard_map/split | solution.py:15
  95.2 204.8 %while.15 = (s32[]{:T(128)}, f32[1024,1,2]{0,2,1:T(2,128)S(1)}, f32[1024,1,2]{0,2,1:T(2,128)S(1)}, f32[1024,1,2,128]{0,3,2,1:T(8,128)S(1)}, bf16[16,1024,128]{2,...) while((s32[]{:T(128)}, f32[1024,1,2]{0,2,1:T(2,128)S(1)}, ...), condition=%wide.region_5.6_spmd.clone, body=%wide.region_2.5_spmd.clone.sunk | while | flops 1091317760 | bytes 61998208 | solution.py:104
  95.2 5.4 %bitcast_reduce_fusion.2 = (f32[1024,2]{0,1:T(2,128)S(1)}, f32[1024,1024,2]{1,0,2:T(8,128)}) fusion(bf16[1024,1,2,128]{3,0,2,1:T(8,128)(2,1)S(1)} %get-tuple-element.203, bf16[16,1024,128]{2,1,0:T(8,128)(2,1)} %get-tuple-element.202, s32[]{:T(128)} %get-tuple-element.189), kind=kOutput, calls=%fused_computation.1.clone.1 | convolution fusion | flops 541063168 | bytes 9183744 | tf_op jit(solution)/shard_map/while/body/eval_jaxpr/tkgd,rkd->tkgr/dot_general | solution.py:54
  100.6 5.6 %fusion.61 = f32[1024,1,2,128]{0,3,2,1:T(8,128)S(1)} fusion(f32[1024,1024,2]{1,0,2:T(8,128)} %get-tuple-element.178, f32[1024,2]{0,1:T(2,128)S(1)} %bitcast.126, f32[1024,1,2,128]{0,3,2,1:T(8,128)S(1)} %get-tuple-element.192, f32[1024,2]{0,1:T(2,128)S(1)} %get-tuple-element.179, pred[]{:T(512)S(6)} %compare.14, ...), kind=kOutput, calls=%fused_computation.10.clone.1 | convolution fusion | flops 543948800 | bytes 10764801 | tf_op jit(solution)/shard_map/while/body/eval_jaxpr/tkgr,rkd->tkgd/dot_general | solution.py:61
  106.6 1.4 fusion.60
  108.0 5.4 %bitcast_reduce_fusion.2 = (f32[1024,2]{0,1:T(2,128)S(1)}, f32[1024,1024,2]{1,0,2:T(8,128)}) fusion(bf16[1024,1,2,128]{3,0,2,1:T(8,128)(2,1)S(1)} %get-tuple-element.203, bf16[16,1024,128]{2,1,0:T(8,128)(2,1)} %get-tuple-element.202, s32[]{:T(128)} %get-tuple-element.189), kind=kOutput, calls=%fused_computation.1.clone.1 | convolution fusion | flops 541063168 | bytes 9183744 | tf_op jit(solution)/shard_map/while/body/eval_jaxpr/tkgd,rkd->tkgr/dot_general | solution.py:54
  113.5 5.5 %fusion.61 = f32[1024,1,2,128]{0,3,2,1:T(8,128)S(1)} fusion(f32[1024,1024,2]{1,0,2:T(8,128)} %get-tuple-element.178, f32[1024,2]{0,1:T(2,128)S(1)} %bitcast.126, f32[1024,1,2,128]{0,3,2,1:T(8,128)S(1)} %get-tuple-element.192, f32[1024,2]{0,1:T(2,128)S(1)} %get-tuple-element.179, pred[]{:T(512)S(6)} %compare.14, ...), kind=kOutput, calls=%fused_computation.10.clone.1 | convolution fusion | flops 543948800 | bytes 10764801 | tf_op jit(solution)/shard_map/while/body/eval_jaxpr/tkgr,rkd->tkgd/dot_general | solution.py:61
  119.3 1.4 fusion.60
  120.8 5.4 %bitcast_reduce_fusion.2 = (f32[1024,2]{0,1:T(2,128)S(1)}, f32[1024,1024,2]{1,0,2:T(8,128)}) fusion(bf16[1024,1,2,128]{3,0,2,1:T(8,128)(2,1)S(1)} %get-tuple-element.203, bf16[16,1024,128]{2,1,0:T(8,128)(2,1)} %get-tuple-element.202, s32[]{:T(128)} %get-tuple-element.189), kind=kOutput, calls=%fused_computation.1.clone.1 | convolution fusion | flops 541063168 | bytes 9183744 | tf_op jit(solution)/shard_map/while/body/eval_jaxpr/tkgd,rkd->tkgr/dot_general | solution.py:54
  126.2 5.5 %fusion.61 = f32[1024,1,2,128]{0,3,2,1:T(8,128)S(1)} fusion(f32[1024,1024,2]{1,0,2:T(8,128)} %get-tuple-element.178, f32[1024,2]{0,1:T(2,128)S(1)} %bitcast.126, f32[1024,1,2,128]{0,3,2,1:T(8,128)S(1)} %get-tuple-element.192, f32[1024,2]{0,1:T(2,128)S(1)} %get-tuple-element.179, pred[]{:T(512)S(6)} %compare.14, ...), kind=kOutput, calls=%fused_computation.10.clone.1 | convolution fusion | flops 543948800 | bytes 10764801 | tf_op jit(solution)/shard_map/while/body/eval_jaxpr/tkgr,rkd->tkgd/dot_general | solution.py:61
  132.1 1.4 fusion.60
  133.5 5.4 %bitcast_reduce_fusion.2 = (f32[1024,2]{0,1:T(2,128)S(1)}, f32[1024,1024,2]{1,0,2:T(8,128)}) fusion(bf16[1024,1,2,128]{3,0,2,1:T(8,128)(2,1)S(1)} %get-tuple-element.203, bf16[16,1024,128]{2,1,0:T(8,128)(2,1)} %get-tuple-element.202, s32[]{:T(128)} %get-tuple-element.189), kind=kOutput, calls=%fused_computation.1.clone.1 | convolution fusion | flops 541063168 | bytes 9183744 | tf_op jit(solution)/shard_map/while/body/eval_jaxpr/tkgd,rkd->tkgr/dot_general | solution.py:54
  139.0 5.6 %fusion.61 = f32[1024,1,2,128]{0,3,2,1:T(8,128)S(1)} fusion(f32[1024,1024,2]{1,0,2:T(8,128)} %get-tuple-element.178, f32[1024,2]{0,1:T(2,128)S(1)} %bitcast.126, f32[1024,1,2,128]{0,3,2,1:T(8,128)S(1)} %get-tuple-element.192, f32[1024,2]{0,1:T(2,128)S(1)} %get-tuple-element.179, pred[]{:T(512)S(6)} %compare.14, ...), kind=kOutput, calls=%fused_computation.10.clone.1 | convolution fusion | flops 543948800 | bytes 10764801 | tf_op jit(solution)/shard_map/while/body/eval_jaxpr/tkgr,rkd->tkgd/dot_general | solution.py:61
  145.1 1.4 fusion.60
  146.6 5.4 %bitcast_reduce_fusion.2 = (f32[1024,2]{0,1:T(2,128)S(1)}, f32[1024,1024,2]{1,0,2:T(8,128)}) fusion(bf16[1024,1,2,128]{3,0,2,1:T(8,128)(2,1)S(1)} %get-tuple-element.203, bf16[16,1024,128]{2,1,0:T(8,128)(2,1)} %get-tuple-element.202, s32[]{:T(128)} %get-tuple-element.189), kind=kOutput, calls=%fused_computation.1.clone.1 | convolution fusion | flops 541063168 | bytes 9183744 | tf_op jit(solution)/shard_map/while/body/eval_jaxpr/tkgd,rkd->tkgr/dot_general | solution.py:54
  152.0 5.5 %fusion.61 = f32[1024,1,2,128]{0,3,2,1:T(8,128)S(1)} fusion(f32[1024,1024,2]{1,0,2:T(8,128)} %get-tuple-element.178, f32[1024,2]{0,1:T(2,128)S(1)} %bitcast.126, f32[1024,1,2,128]{0,3,2,1:T(8,128)S(1)} %get-tuple-element.192, f32[1024,2]{0,1:T(2,128)S(1)} %get-tuple-element.179, pred[]{:T(512)S(6)} %compare.14, ...), kind=kOutput, calls=%fused_computation.10.clone.1 | convolution fusion | flops 543948800 | bytes 10764801 | tf_op jit(solution)/shard_map/while/body/eval_jaxpr/tkgr,rkd->tkgd/dot_general | solution.py:61
  157.9 1.4 fusion.60
  159.3 5.4 %bitcast_reduce_fusion.2 = (f32[1024,2]{0,1:T(2,128)S(1)}, f32[1024,1024,2]{1,0,2:T(8,128)}) fusion(bf16[1024,1,2,128]{3,0,2,1:T(8,128)(2,1)S(1)} %get-tuple-element.203, bf16[16,1024,128]{2,1,0:T(8,128)(2,1)} %get-tuple-element.202, s32[]{:T(128)} %get-tuple-element.189), kind=kOutput, calls=%fused_computation.1.clone.1 | convolution fusion | flops 541063168 | bytes 9183744 | tf_op jit(solution)/shard_map/while/body/eval_jaxpr/tkgd,rkd->tkgr/dot_general | solution.py:54
  164.8 5.6 %fusion.61 = f32[1024,1,2,128]{0,3,2,1:T(8,128)S(1)} fusion(f32[1024,1024,2]{1,0,2:T(8,128)} %get-tuple-element.178, f32[1024,2]{0,1:T(2,128)S(1)} %bitcast.126, f32[1024,1,2,128]{0,3,2,1:T(8,128)S(1)} %get-tuple-element.192, f32[1024,2]{0,1:T(2,128)S(1)} %get-tuple-element.179, pred[]{:T(512)S(6)} %compare.14, ...), kind=kOutput, calls=%fused_computation.10.clone.1 | convolution fusion | flops 543948800 | bytes 10764801 | tf_op jit(solution)/shard_map/while/body/eval_jaxpr/tkgr,rkd->tkgd/dot_general | solution.py:61
  170.7 1.4 fusion.60
  172.1 5.4 %bitcast_reduce_fusion.2 = (f32[1024,2]{0,1:T(2,128)S(1)}, f32[1024,1024,2]{1,0,2:T(8,128)}) fusion(bf16[1024,1,2,128]{3,0,2,1:T(8,128)(2,1)S(1)} %get-tuple-element.203, bf16[16,1024,128]{2,1,0:T(8,128)(2,1)} %get-tuple-element.202, s32[]{:T(128)} %get-tuple-element.189), kind=kOutput, calls=%fused_computation.1.clone.1 | convolution fusion | flops 541063168 | bytes 9183744 | tf_op jit(solution)/shard_map/while/body/eval_jaxpr/tkgd,rkd->tkgr/dot_general | solution.py:54
  177.6 5.8 %fusion.61 = f32[1024,1,2,128]{0,3,2,1:T(8,128)S(1)} fusion(f32[1024,1024,2]{1,0,2:T(8,128)} %get-tuple-element.178, f32[1024,2]{0,1:T(2,128)S(1)} %bitcast.126, f32[1024,1,2,128]{0,3,2,1:T(8,128)S(1)} %get-tuple-element.192, f32[1024,2]{0,1:T(2,128)S(1)} %get-tuple-element.179, pred[]{:T(512)S(6)} %compare.14, ...), kind=kOutput, calls=%fused_computation.10.clone.1 | convolution fusion | flops 543948800 | bytes 10764801 | tf_op jit(solution)/shard_map/while/body/eval_jaxpr/tkgr,rkd->tkgd/dot_general | solution.py:61
  183.8 1.4 fusion.60
  185.2 5.4 %bitcast_reduce_fusion.2 = (f32[1024,2]{0,1:T(2,128)S(1)}, f32[1024,1024,2]{1,0,2:T(8,128)}) fusion(bf16[1024,1,2,128]{3,0,2,1:T(8,128)(2,1)S(1)} %get-tuple-element.203, bf16[16,1024,128]{2,1,0:T(8,128)(2,1)} %get-tuple-element.202, s32[]{:T(128)} %get-tuple-element.189), kind=kOutput, calls=%fused_computation.1.clone.1 | convolution fusion | flops 541063168 | bytes 9183744 | tf_op jit(solution)/shard_map/while/body/eval_jaxpr/tkgd,rkd->tkgr/dot_general | solution.py:54
  190.7 5.6 %fusion.61 = f32[1024,1,2,128]{0,3,2,1:T(8,128)S(1)} fusion(f32[1024,1024,2]{1,0,2:T(8,128)} %get-tuple-element.178, f32[1024,2]{0,1:T(2,128)S(1)} %bitcast.126, f32[1024,1,2,128]{0,3,2,1:T(8,128)S(1)} %get-tuple-element.192, f32[1024,2]{0,1:T(2,128)S(1)} %get-tuple-element.179, pred[]{:T(512)S(6)} %compare.14, ...), kind=kOutput, calls=%fused_computation.10.clone.1 | convolution fusion | flops 543948800 | bytes 10764801 | tf_op jit(solution)/shard_map/while/body/eval_jaxpr/tkgr,rkd->tkgd/dot_general | solution.py:61
  196.8 1.4 fusion.60
  198.2 5.4 %bitcast_reduce_fusion.2 = (f32[1024,2]{0,1:T(2,128)S(1)}, f32[1024,1024,2]{1,0,2:T(8,128)}) fusion(bf16[1024,1,2,128]{3,0,2,1:T(8,128)(2,1)S(1)} %get-tuple-element.203, bf16[16,1024,128]{2,1,0:T(8,128)(2,1)} %get-tuple-element.202, s32[]{:T(128)} %get-tuple-element.189), kind=kOutput, calls=%fused_computation.1.clone.1 | convolution fusion | flops 541063168 | bytes 9183744 | tf_op jit(solution)/shard_map/while/body/eval_jaxpr/tkgd,rkd->tkgr/dot_general | solution.py:54
  203.7 5.5 %fusion.61 = f32[1024,1,2,128]{0,3,2,1:T(8,128)S(1)} fusion(f32[1024,1024,2]{1,0,2:T(8,128)} %get-tuple-element.178, f32[1024,2]{0,1:T(2,128)S(1)} %bitcast.126, f32[1024,1,2,128]{0,3,2,1:T(8,128)S(1)} %get-tuple-element.192, f32[1024,2]{0,1:T(2,128)S(1)} %get-tuple-element.179, pred[]{:T(512)S(6)} %compare.14, ...), kind=kOutput, calls=%fused_computation.10.clone.1 | convolution fusion | flops 543948800 | bytes 10764801 | tf_op jit(solution)/shard_map/while/body/eval_jaxpr/tkgr,rkd->tkgd/dot_general | solution.py:61
  209.5 1.4 fusion.60
  210.9 5.4 %bitcast_reduce_fusion.2 = (f32[1024,2]{0,1:T(2,128)S(1)}, f32[1024,1024,2]{1,0,2:T(8,128)}) fusion(bf16[1024,1,2,128]{3,0,2,1:T(8,128)(2,1)S(1)} %get-tuple-element.203, bf16[16,1024,128]{2,1,0:T(8,128)(2,1)} %get-tuple-element.202, s32[]{:T(128)} %get-tuple-element.189), kind=kOutput, calls=%fused_computation.1.clone.1 | convolution fusion | flops 541063168 | bytes 9183744 | tf_op jit(solution)/shard_map/while/body/eval_jaxpr/tkgd,rkd->tkgr/dot_general | solution.py:54
  216.4 5.5 %fusion.61 = f32[1024,1,2,128]{0,3,2,1:T(8,128)S(1)} fusion(f32[1024,1024,2]{1,0,2:T(8,128)} %get-tuple-element.178, f32[1024,2]{0,1:T(2,128)S(1)} %bitcast.126, f32[1024,1,2,128]{0,3,2,1:T(8,128)S(1)} %get-tuple-element.192, f32[1024,2]{0,1:T(2,128)S(1)} %get-tuple-element.179, pred[]{:T(512)S(6)} %compare.14, ...), kind=kOutput, calls=%fused_computation.10.clone.1 | convolution fusion | flops 543948800 | bytes 10764801 | tf_op jit(solution)/shard_map/while/body/eval_jaxpr/tkgr,rkd->tkgd/dot_general | solution.py:61
  222.2 1.4 fusion.60
  223.7 5.4 %bitcast_reduce_fusion.2 = (f32[1024,2]{0,1:T(2,128)S(1)}, f32[1024,1024,2]{1,0,2:T(8,128)}) fusion(bf16[1024,1,2,128]{3,0,2,1:T(8,128)(2,1)S(1)} %get-tuple-element.203, bf16[16,1024,128]{2,1,0:T(8,128)(2,1)} %get-tuple-element.202, s32[]{:T(128)} %get-tuple-element.189), kind=kOutput, calls=%fused_computation.1.clone.1 | convolution fusion | flops 541063168 | bytes 9183744 | tf_op jit(solution)/shard_map/while/body/eval_jaxpr/tkgd,rkd->tkgr/dot_general | solution.py:54
  229.1 5.5 %fusion.61 = f32[1024,1,2,128]{0,3,2,1:T(8,128)S(1)} fusion(f32[1024,1024,2]{1,0,2:T(8,128)} %get-tuple-element.178, f32[1024,2]{0,1:T(2,128)S(1)} %bitcast.126, f32[1024,1,2,128]{0,3,2,1:T(8,128)S(1)} %get-tuple-element.192, f32[1024,2]{0,1:T(2,128)S(1)} %get-tuple-element.179, pred[]{:T(512)S(6)} %compare.14, ...), kind=kOutput, calls=%fused_computation.10.clone.1 | convolution fusion | flops 543948800 | bytes 10764801 | tf_op jit(solution)/shard_map/while/body/eval_jaxpr/tkgr,rkd->tkgd/dot_general | solution.py:61
  235.0 1.4 fusion.60
  236.4 5.4 %bitcast_reduce_fusion.2 = (f32[1024,2]{0,1:T(2,128)S(1)}, f32[1024,1024,2]{1,0,2:T(8,128)}) fusion(bf16[1024,1,2,128]{3,0,2,1:T(8,128)(2,1)S(1)} %get-tuple-element.203, bf16[16,1024,128]{2,1,0:T(8,128)(2,1)} %get-tuple-element.202, s32[]{:T(128)} %get-tuple-element.189), kind=kOutput, calls=%fused_computation.1.clone.1 | convolution fusion | flops 541063168 | bytes 9183744 | tf_op jit(solution)/shard_map/while/body/eval_jaxpr/tkgd,rkd->tkgr/dot_general | solution.py:54
  241.8 5.5 %fusion.61 = f32[1024,1,2,128]{0,3,2,1:T(8,128)S(1)} fusion(f32[1024,1024,2]{1,0,2:T(8,128)} %get-tuple-element.178, f32[1024,2]{0,1:T(2,128)S(1)} %bitcast.126, f32[1024,1,2,128]{0,3,2,1:T(8,128)S(1)} %get-tuple-element.192, f32[1024,2]{0,1:T(2,128)S(1)} %get-tuple-element.179, pred[]{:T(512)S(6)} %compare.14, ...), kind=kOutput, calls=%fused_computation.10.clone.1 | convolution fusion | flops 543948800 | bytes 10764801 | tf_op jit(solution)/shard_map/while/body/eval_jaxpr/tkgr,rkd->tkgd/dot_general | solution.py:61
  247.7 1.4 fusion.60
  249.1 5.4 %bitcast_reduce_fusion.2 = (f32[1024,2]{0,1:T(2,128)S(1)}, f32[1024,1024,2]{1,0,2:T(8,128)}) fusion(bf16[1024,1,2,128]{3,0,2,1:T(8,128)(2,1)S(1)} %get-tuple-element.203, bf16[16,1024,128]{2,1,0:T(8,128)(2,1)} %get-tuple-element.202, s32[]{:T(128)} %get-tuple-element.189), kind=kOutput, calls=%fused_computation.1.clone.1 | convolution fusion | flops 541063168 | bytes 9183744 | tf_op jit(solution)/shard_map/while/body/eval_jaxpr/tkgd,rkd->tkgr/dot_general | solution.py:54
  254.6 5.5 %fusion.61 = f32[1024,1,2,128]{0,3,2,1:T(8,128)S(1)} fusion(f32[1024,1024,2]{1,0,2:T(8,128)} %get-tuple-element.178, f32[1024,2]{0,1:T(2,128)S(1)} %bitcast.126, f32[1024,1,2,128]{0,3,2,1:T(8,128)S(1)} %get-tuple-element.192, f32[1024,2]{0,1:T(2,128)S(1)} %get-tuple-element.179, pred[]{:T(512)S(6)} %compare.14, ...), kind=kOutput, calls=%fused_computation.10.clone.1 | convolution fusion | flops 543948800 | bytes 10764801 | tf_op jit(solution)/shard_map/while/body/eval_jaxpr/tkgr,rkd->tkgd/dot_general | solution.py:61
  260.4 1.4 fusion.60
  261.8 5.4 %bitcast_reduce_fusion.2 = (f32[1024,2]{0,1:T(2,128)S(1)}, f32[1024,1024,2]{1,0,2:T(8,128)}) fusion(bf16[1024,1,2,128]{3,0,2,1:T(8,128)(2,1)S(1)} %get-tuple-element.203, bf16[16,1024,128]{2,1,0:T(8,128)(2,1)} %get-tuple-element.202, s32[]{:T(128)} %get-tuple-element.189), kind=kOutput, calls=%fused_computation.1.clone.1 | convolution fusion | flops 541063168 | bytes 9183744 | tf_op jit(solution)/shard_map/while/body/eval_jaxpr/tkgd,rkd->tkgr/dot_general | solution.py:54
  267.3 5.5 %fusion.61 = f32[1024,1,2,128]{0,3,2,1:T(8,128)S(1)} fusion(f32[1024,1024,2]{1,0,2:T(8,128)} %get-tuple-element.178, f32[1024,2]{0,1:T(2,128)S(1)} %bitcast.126, f32[1024,1,2,128]{0,3,2,1:T(8,128)S(1)} %get-tuple-element.192, f32[1024,2]{0,1:T(2,128)S(1)} %get-tuple-element.179, pred[]{:T(512)S(6)} %compare.14, ...), kind=kOutput, calls=%fused_computation.10.clone.1 | convolution fusion | flops 543948800 | bytes 10764801 | tf_op jit(solution)/shard_map/while/body/eval_jaxpr/tkgr,rkd->tkgd/dot_general | solution.py:61
  273.1 1.4 fusion.60
  274.6 5.4 %bitcast_reduce_fusion.2 = (f32[1024,2]{0,1:T(2,128)S(1)}, f32[1024,1024,2]{1,0,2:T(8,128)}) fusion(bf16[1024,1,2,128]{3,0,2,1:T(8,128)(2,1)S(1)} %get-tuple-element.203, bf16[16,1024,128]{2,1,0:T(8,128)(2,1)} %get-tuple-element.202, s32[]{:T(128)} %get-tuple-element.189), kind=kOutput, calls=%fused_computation.1.clone.1 | convolution fusion | flops 541063168 | bytes 9183744 | tf_op jit(solution)/shard_map/while/body/eval_jaxpr/tkgd,rkd->tkgr/dot_general | solution.py:54
  280.0 5.5 %fusion.61 = f32[1024,1,2,128]{0,3,2,1:T(8,128)S(1)} fusion(f32[1024,1024,2]{1,0,2:T(8,128)} %get-tuple-element.178, f32[1024,2]{0,1:T(2,128)S(1)} %bitcast.126, f32[1024,1,2,128]{0,3,2,1:T(8,128)S(1)} %get-tuple-element.192, f32[1024,2]{0,1:T(2,128)S(1)} %get-tuple-element.179, pred[]{:T(512)S(6)} %compare.14, ...), kind=kOutput, calls=%fused_computation.10.clone.1 | convolution fusion | flops 543948800 | bytes 10764801 | tf_op jit(solution)/shard_map/while/body/eval_jaxpr/tkgr,rkd->tkgd/dot_general | solution.py:61
  285.9 1.4 fusion.60
  287.3 5.4 %bitcast_reduce_fusion.2 = (f32[1024,2]{0,1:T(2,128)S(1)}, f32[1024,1024,2]{1,0,2:T(8,128)}) fusion(bf16[1024,1,2,128]{3,0,2,1:T(8,128)(2,1)S(1)} %get-tuple-element.203, bf16[16,1024,128]{2,1,0:T(8,128)(2,1)} %get-tuple-element.202, s32[]{:T(128)} %get-tuple-element.189), kind=kOutput, calls=%fused_computation.1.clone.1 | convolution fusion | flops 541063168 | bytes 9183744 | tf_op jit(solution)/shard_map/while/body/eval_jaxpr/tkgd,rkd->tkgr/dot_general | solution.py:54
  292.7 5.5 %fusion.61 = f32[1024,1,2,128]{0,3,2,1:T(8,128)S(1)} fusion(f32[1024,1024,2]{1,0,2:T(8,128)} %get-tuple-element.178, f32[1024,2]{0,1:T(2,128)S(1)} %bitcast.126, f32[1024,1,2,128]{0,3,2,1:T(8,128)S(1)} %get-tuple-element.192, f32[1024,2]{0,1:T(2,128)S(1)} %get-tuple-element.179, pred[]{:T(512)S(6)} %compare.14, ...), kind=kOutput, calls=%fused_computation.10.clone.1 | convolution fusion | flops 543948800 | bytes 10764801 | tf_op jit(solution)/shard_map/while/body/eval_jaxpr/tkgr,rkd->tkgd/dot_general | solution.py:61
  298.6 1.4 fusion.60
  300.3 14.4 %all_to_all.19 = bf16[8,128,256]{1,2,0:T(8,128)(2,1)S(1)} all-to-all(bf16[8,128,256]{1,2,0:T(8,128)(2,1)S(1)} %copy.31), channel_id=1, replica_groups=mesh['sp'=16,'tp'=8] {'tp'}, dimensions={0} | all-to-all | bytes 1048576 | tf_op jit(solution)/shard_map/all_to_all | solution.py:107
  314.7 4.8 %multiply_reduce_fusion = (f32[128]{0:T(128)S(1)}, f32[128,2048]{1,0:T(8,128)S(1)}) fusion(bf16[128,2048]{0,1:T(8,128)(2,1)S(1)} %bitcast.128, bf16[2048,2048]{1,0:T(8,128)(2,1)} %param.18, bf16[128,2048]{1,0:T(8,128)(2,1)S(1)} %copy-done.2), kind=kOutput, calls=%fused_computation.38 | convolution fusion | flops 1074790272 | bytes 10486272 | tf_op jit(solution)/shard_map/dot_general | solution.py:108
  319.5 1.0 multiply_convert_fusion.1
  320.8 29.9 %all-gather.7.cloned.1.call-done = bf16[1024,2048]{1,0:T(8,128)(2,1)} async-done(((bf16[128,2048]{1,0:T(8,128)(2,1)}), bf16[1024,2048]{1,0:T(8,128)(2,1)}) %all-gather.7.cloned.1.call-update) | async-done | bytes 4194320 | tf_op jit(solution)/shard_map/all_gather | solution.py:113
  350.7 14.4 %convolution_convert_fusion = bf16[1024,2048]{1,0:T(8,128)(2,1)} fusion(bf16[1024,2048]{1,0:T(8,128)(2,1)} %all-gather.11.cloned.1.call-done, bf16[1024,2048]{1,0:T(8,128)(2,1)} %all-gather.7.cloned.1.call-done, bf16[2048,1024]{1,0:T(8,128)(2,1)} %all-gather.9.cloned.1.call-done), kind=kOutput, calls=%fused_computation.28 | convolution fusion | flops 8595177472 | bytes 16777216 | tf_op jit(solution)/shard_map/dot_general | solution.py:124
  365.1 38.0 %reduce-scatter.2.cloned.1.call-done = bf16[128,2048]{1,0:T(8,128)(2,1)} async-done(((bf16[1024,2048]{1,0:T(8,128)(2,1)}), bf16[128,2048]{1,0:T(8,128)(2,1)}) %reduce-scatter.2.cloned.1.call-update) | async-done | bytes 524304 | tf_op jit(solution)/shard_map/reduce_scatter | solution.py:123
  403.1 1.9 add_convert_fusion
  (125 shorter events, 12.4 us)
Async XLA Ops:
  6.5 4.4 %copy-start.1 = (bf16[1024,128]{1,0:T(8,128)(2,1)S(1)}, bf16[1024,128]{1,0:T(8,128)(2,1)}, u32[]{:S(2)}) copy-start(bf16[1024,128]{1,0:T(8,128)(2,1)} %param.14) | copy-start | bytes 786436
  6.5 4.4 %copy-start.5 = (f32[128]{0:T(128)S(1)}, f32[128]{0:T(128)}, u32[]{:S(2)}) copy-start(f32[128]{0:T(128)} %param.17) | copy-start | bytes 1540
  6.5 82.9 %all-gather.5.cloned.1.call-start = ((), (), s32[]{:S(2)}) async-start(), calls=%async_computation.2 | async-start | bytes 8912896 | tf_op jit(solution)/shard_map/all_gather | solution.py:14
  8.9 6.1 %copy-start.3 = (bf16[1024,128]{1,0:T(8,128)(2,1)S(1)}, bf16[1024,128]{1,0:T(8,128)(2,1)}, u32[]{:S(2)}) copy-start(bf16[1024,128]{1,0:T(8,128)(2,1)} %param.15) | copy-start | bytes 786436
  10.9 8.2 %copy-start.6 = (f32[128]{0:T(128)S(1)}, f32[128]{0:T(128)}, u32[]{:S(2)}) copy-start(f32[128]{0:T(128)} %param.16) | copy-start | bytes 1540
  15.9 304.9 %all-gather.11.cloned.1.call-start = ((), (), s32[]{:S(2)}) async-start(), calls=%async_computation.5 | async-start | bytes 4456448 | tf_op jit(solution)/shard_map/all_gather | solution.py:122
  16.6 304.2 %all-gather.9.cloned.1.call-start = ((), (), s32[]{:S(2)}) async-start(), calls=%async_computation.4 | async-start | bytes 4456448 | tf_op jit(solution)/shard_map/all_gather | solution.py:117
  17.4 333.3 %all-gather.7.cloned.1.call-start = ((), (), s32[]{:S(2)}) async-start(), calls=%async_computation.3 | async-start | bytes 4718592 | tf_op jit(solution)/shard_map/all_gather | solution.py:113
  100.6 6.0 %copy-start = (f32[1024,1024,2]{1,0,2:T(8,128)S(1)}, f32[1024,1024,2]{1,0,2:T(8,128)}, u32[]{:S(2)}) copy-start(f32[1024,1024,2]{1,0,2:T(8,128)} %get-tuple-element.178) | copy-start | bytes 25165828 | tf_op jit(solution)/shard_map/while
  113.5 5.8 %copy-start = (f32[1024,1024,2]{1,0,2:T(8,128)S(1)}, f32[1024,1024,2]{1,0,2:T(8,128)}, u32[]{:S(2)}) copy-start(f32[1024,1024,2]{1,0,2:T(8,128)} %get-tuple-element.178) | copy-start | bytes 25165828 | tf_op jit(solution)/shard_map/while
  126.2 5.8 %copy-start = (f32[1024,1024,2]{1,0,2:T(8,128)S(1)}, f32[1024,1024,2]{1,0,2:T(8,128)}, u32[]{:S(2)}) copy-start(f32[1024,1024,2]{1,0,2:T(8,128)} %get-tuple-element.178) | copy-start | bytes 25165828 | tf_op jit(solution)/shard_map/while
  138.9 6.2 %copy-start = (f32[1024,1024,2]{1,0,2:T(8,128)S(1)}, f32[1024,1024,2]{1,0,2:T(8,128)}, u32[]{:S(2)}) copy-start(f32[1024,1024,2]{1,0,2:T(8,128)} %get-tuple-element.178) | copy-start | bytes 25165828 | tf_op jit(solution)/shard_map/while
  152.0 5.8 %copy-start = (f32[1024,1024,2]{1,0,2:T(8,128)S(1)}, f32[1024,1024,2]{1,0,2:T(8,128)}, u32[]{:S(2)}) copy-start(f32[1024,1024,2]{1,0,2:T(8,128)} %get-tuple-element.178) | copy-start | bytes 25165828 | tf_op jit(solution)/shard_map/while
  164.7 6.0 %copy-start = (f32[1024,1024,2]{1,0,2:T(8,128)S(1)}, f32[1024,1024,2]{1,0,2:T(8,128)}, u32[]{:S(2)}) copy-start(f32[1024,1024,2]{1,0,2:T(8,128)} %get-tuple-element.178) | copy-start | bytes 25165828 | tf_op jit(solution)/shard_map/while
  177.6 6.2 %copy-start = (f32[1024,1024,2]{1,0,2:T(8,128)S(1)}, f32[1024,1024,2]{1,0,2:T(8,128)}, u32[]{:S(2)}) copy-start(f32[1024,1024,2]{1,0,2:T(8,128)} %get-tuple-element.178) | copy-start | bytes 25165828 | tf_op jit(solution)/shard_map/while
  190.6 6.1 %copy-start = (f32[1024,1024,2]{1,0,2:T(8,128)S(1)}, f32[1024,1024,2]{1,0,2:T(8,128)}, u32[]{:S(2)}) copy-start(f32[1024,1024,2]{1,0,2:T(8,128)} %get-tuple-element.178) | copy-start | bytes 25165828 | tf_op jit(solution)/shard_map/while
  203.7 5.8 %copy-start = (f32[1024,1024,2]{1,0,2:T(8,128)S(1)}, f32[1024,1024,2]{1,0,2:T(8,128)}, u32[]{:S(2)}) copy-start(f32[1024,1024,2]{1,0,2:T(8,128)} %get-tuple-element.178) | copy-start | bytes 25165828 | tf_op jit(solution)/shard_map/while
  216.4 5.8 %copy-start = (f32[1024,1024,2]{1,0,2:T(8,128)S(1)}, f32[1024,1024,2]{1,0,2:T(8,128)}, u32[]{:S(2)}) copy-start(f32[1024,1024,2]{1,0,2:T(8,128)} %get-tuple-element.178) | copy-start | bytes 25165828 | tf_op jit(solution)/shard_map/while
  229.1 5.8 %copy-start = (f32[1024,1024,2]{1,0,2:T(8,128)S(1)}, f32[1024,1024,2]{1,0,2:T(8,128)}, u32[]{:S(2)}) copy-start(f32[1024,1024,2]{1,0,2:T(8,128)} %get-tuple-element.178) | copy-start | bytes 25165828 | tf_op jit(solution)/shard_map/while
  241.8 5.8 %copy-start = (f32[1024,1024,2]{1,0,2:T(8,128)S(1)}, f32[1024,1024,2]{1,0,2:T(8,128)}, u32[]{:S(2)}) copy-start(f32[1024,1024,2]{1,0,2:T(8,128)} %get-tuple-element.178) | copy-start | bytes 25165828 | tf_op jit(solution)/shard_map/while
  254.6 5.8 %copy-start = (f32[1024,1024,2]{1,0,2:T(8,128)S(1)}, f32[1024,1024,2]{1,0,2:T(8,128)}, u32[]{:S(2)}) copy-start(f32[1024,1024,2]{1,0,2:T(8,128)} %get-tuple-element.178) | copy-start | bytes 25165828 | tf_op jit(solution)/shard_map/while
  267.3 5.8 %copy-start = (f32[1024,1024,2]{1,0,2:T(8,128)S(1)}, f32[1024,1024,2]{1,0,2:T(8,128)}, u32[]{:S(2)}) copy-start(f32[1024,1024,2]{1,0,2:T(8,128)} %get-tuple-element.178) | copy-start | bytes 25165828 | tf_op jit(solution)/shard_map/while
  280.0 5.8 %copy-start = (f32[1024,1024,2]{1,0,2:T(8,128)S(1)}, f32[1024,1024,2]{1,0,2:T(8,128)}, u32[]{:S(2)}) copy-start(f32[1024,1024,2]{1,0,2:T(8,128)} %get-tuple-element.178) | copy-start | bytes 25165828 | tf_op jit(solution)/shard_map/while
  292.7 5.8 %copy-start = (f32[1024,1024,2]{1,0,2:T(8,128)S(1)}, f32[1024,1024,2]{1,0,2:T(8,128)}, u32[]{:S(2)}) copy-start(f32[1024,1024,2]{1,0,2:T(8,128)} %get-tuple-element.178) | copy-start | bytes 25165828 | tf_op jit(solution)/shard_map/while
  300.0 14.7 %copy-start.2 = (bf16[128,2048]{1,0:T(8,128)(2,1)S(1)}, bf16[128,2048]{1,0:T(8,128)(2,1)}, u32[]{:S(2)}) copy-start(bf16[128,2048]{1,0:T(8,128)(2,1)} %param.12) | copy-start | bytes 1572868
  314.7 4.8 %copy-start.4 = (f32[2048]{0:T(1024)S(1)}, f32[2048]{0:T(1024)}, u32[]{:S(2)}) copy-start(f32[2048]{0:T(1024)} %param.19) | copy-start | bytes 24580
  320.5 82.6 %reduce-scatter.2.cloned.1.call-start = ((), (), s32[]{:S(2)}) async-start(), calls=%async_computation.6 | async-start | bytes 4718592 | tf_op jit(solution)/shard_map/reduce_scatter | solution.py:123
Sparse Core Ops, SparseCore 0:
  16.0 73.4 all-gather.4
  91.6 56.5 all-gather.10
  150.3 50.7 all-gather.8
  320.6 29.9 all-gather.6
  365.2 37.8 reduce-scatter.1
where the time goes:
time: 412 us
  matrix products  194 us (47%)
  waiting for transfers between devices  137 us (33%)
  other arithmetic  37.7 us (9%)
  blocking collectives  14.4 us (3%)
  local copies, waits for them, and re-layouts  14.1 us (3%)
  between operations  13.4 us (3%)
    dot_general x16, matrix products, attend(): jnp.einsum('tkgr,rkd->tkgd', weights.astype(jnp.bfloat16), value_lattice,...  88.3 us
    dot_general x16, matrix products, attend(): jnp.einsum('tkgd,rkd->tkgr', query_grid, key_lattice, preferred_element_t...  86.8 us
    all_gather x1, waiting for transfers between devices, sent_together(): filled = lax.all_gather(both, axis, axis=dim, tiled=True)  67.3 us
    reduce_scatter x1, waiting for transfers between devices, local(): lax.psum_scatter(jnp.dot(act, down_whole, preferred_element_type=jnp.floa...  38 us
    all_gather x1, waiting for transfers between devices, local(): whole_rows = lax.all_gather(normed, 'tp', axis=0, tiled=True)  29.9 us
    reduce_sum x16, other arithmetic, attend(): mass = mass * factor + jnp.sum(weights, axis=-1)  22.1 us
    all_to_all x1, blocking collectives, local(): lax.all_to_all(attn, 'tp', split_axis=0, concat_axis=1, tiled=True)  14.4 us
    dot_general x1, matrix products, local(): jnp.dot(act, down_whole, preferred_element_type=jnp.float32)  14.4 us
  transfers between devices with their start and end apart: 5, of which 3 were waited for; matrix products, arithmetic and copies ran while one was open for 52% of the time, Pallas kernels for 0%

commit v1 on v0

--- a/solution.py
+++ b/solution.py
@@ -110,7 +110,10 @@
     normed = (
         middle * lax.rsqrt(jnp.mean(middle * middle, axis=-1, keepdims=True) + epsilon) * norm_gain
     ).astype(jnp.bfloat16)
-    whole_rows = lax.all_gather(normed, "tp", axis=0, tiled=True)
+    n_dev = lax.axis_size("tp")
+    blocks = jnp.stack([normed for _ in range(n_dev)])
+    blocks = lax.all_to_all(blocks, "tp", split_axis=0, concat_axis=0)
+    whole_rows = jnp.concatenate(blocks, axis=0)
     hidden = jax.nn.relu(
         jnp.dot(
             whole_rows,

time: 412 us -> 436 us (1.058)
  waiting for transfers between devices: 137 us -> 154 us
  starting transfers between devices: 0.34 us -> 4.85 us
    all_to_all x0 -> x1, waiting for transfers between devices: none -> 49.4 us  [local(): blocks = lax.all_to_all(blocks, 'tp', split_axis=0, concat_axis=0)]
    all_gather x1 -> x0, waiting for transfers between devices: 29.9 us -> none  [local(): whole_rows = lax.all_gather(normed, 'tp', axis=0, tiled=True)]
    all_to_all x0 -> x1, starting transfers between devices: none -> 4.55 us  [local(): blocks = lax.all_to_all(blocks, 'tp', split_axis=0, concat_axis=0)]
  transfers between devices with their start and end apart: 5 -> 5, of which waited for: 3 -> 3; matrix products, arithmetic and copies ran while one was open for 52% -> 50% of each run, Pallas kernels for 0% -> 0%
where the time goes in v1:
time: 436 us; the launch traced here: 435 us
  matrix products  194 us (44%)
  waiting for transfers between devices  154 us (35%)
  other arithmetic  36.9 us (8%)
  local copies, waits for them, and re-layouts  16.7 us (4%)
  blocking collectives  14.4 us (3%)
  between operations  13.4 us (3%)
  starting transfers between devices  4.85 us (1%)
    dot_general x16, matrix products, attend(): jnp.einsum('tkgr,rkd->tkgd', weights.astype(jnp.bfloat16), value_lattice,...  88 us
    dot_general x16, matrix products, attend(): jnp.einsum('tkgd,rkd->tkgr', query_grid, key_lattice, preferred_element_t...  86.9 us
    all_gather x1, waiting for transfers between devices, sent_together(): filled = lax.all_gather(both, axis, axis=dim, tiled=True)  67.3 us
    all_to_all x1, waiting for transfers between devices, local(): blocks = lax.all_to_all(blocks, 'tp', split_axis=0, concat_axis=0)  49.4 us
    reduce_scatter x1, waiting for transfers between devices, local(): lax.psum_scatter(jnp.dot(act, down_whole, preferred_element_type=jnp.floa...  36.3 us
    reduce_sum x16, other arithmetic, attend(): mass = mass * factor + jnp.sum(weights, axis=-1)  22.1 us
    all_to_all x1, blocking collectives, local(): lax.all_to_all(attn, 'tp', split_axis=0, concat_axis=1, tiled=True)  14.4 us
    dot_general x1, matrix products, local(): jnp.dot(act, down_whole, preferred_element_type=jnp.float32)  14.4 us
  transfers between devices with their start and end apart: 5, of which 3 were waited for; matrix products, arithmetic and copies ran while one was open for 50% of the time, Pallas kernels for 0%

profile of v1, /device:TPU:0, one launch (start us, length us, event | category | flops | bytes accessed | tf_op | source)
XLA Modules:
  0.0 435.4 jit_solution(7121753132566006017)
XLA Ops:
  6.6 1.2 fusion.26
  9.0 1.6 fusion.33
  10.9 4.1 fusion.31
  17.6 1.3 copy.26
  20.4 1.2 maximum_multiply_fusion
  22.1 67.3 %all-gather.4.cloned.1.call-done = bf16[16384,256]{1,0:T(8,128)(2,1)} async-done(((bf16[1024,256]{1,0:T(8,128)(2,1)}), bf16[16384,256]{1,0:T(8,128)(2,1)}) %all-gather.4.cloned.1.call-update) | async-done | bytes 8388624 | tf_op jit(solution)/shard_map/all_gather | solution.py:14
  89.5 5.7 %fusion.46 = (bf16[16384,128]{1,0:T(8,128)(2,1)}, bf16[16384,128]{1,0:T(8,128)(2,1)}) fusion(bf16[16384,256]{1,0:T(8,128)(2,1)} %all-gather.4.cloned.1.call-done), kind=kLoop, calls=%fused_computation.85 | loop fusion | bytes 16777216 | tf_op jit(solution)/shard_map/split | solution.py:15
  95.2 204.7 %while.15 = (s32[]{:T(128)}, f32[1024,1,2]{0,2,1:T(2,128)S(1)}, f32[1024,1,2]{0,2,1:T(2,128)S(1)}, f32[1024,1,2,128]{0,3,2,1:T(8,128)S(1)}, bf16[16,1024,128]{2,...) while((s32[]{:T(128)}, f32[1024,1,2]{0,2,1:T(2,128)S(1)}, ...), condition=%wide.region_5.6_spmd.clone, body=%wide.region_2.5_spmd.clone.sunk | while | flops 1091317760 | bytes 61998208 | solution.py:104
  95.2 5.4 %bitcast_reduce_fusion.2 = (f32[1024,2]{0,1:T(2,128)S(1)}, f32[1024,1024,2]{1,0,2:T(8,128)}) fusion(bf16[1024,1,2,128]{3,0,2,1:T(8,128)(2,1)S(1)} %get-tuple-element.203, bf16[16,1024,128]{2,1,0:T(8,128)(2,1)} %get-tuple-element.202, s32[]{:T(128)} %get-tuple-element.189), kind=kOutput, calls=%fused_computation.1.clone.1 | convolution fusion | flops 541063168 | bytes 9183744 | tf_op jit(solution)/shard_map/while/body/eval_jaxpr/tkgd,rkd->tkgr/dot_general | solution.py:54
  100.6 5.6 %fusion.61 = f32[1024,1,2,128]{0,3,2,1:T(8,128)S(1)} fusion(f32[1024,1024,2]{1,0,2:T(8,128)} %get-tuple-element.178, f32[1024,2]{0,1:T(2,128)S(1)} %bitcast.127, f32[1024,1,2,128]{0,3,2,1:T(8,128)S(1)} %get-tuple-element.192, f32[1024,2]{0,1:T(2,128)S(1)} %get-tuple-element.179, pred[]{:T(512)S(6)} %compare.14, ...), kind=kOutput, calls=%fused_computation.10.clone.1 | convolution fusion | flops 543948800 | bytes 10764801 | tf_op jit(solution)/shard_map/while/body/eval_jaxpr/tkgr,rkd->tkgd/dot_general | solution.py:61
  106.6 1.4 fusion.60
  108.1 5.4 %bitcast_reduce_fusion.2 = (f32[1024,2]{0,1:T(2,128)S(1)}, f32[1024,1024,2]{1,0,2:T(8,128)}) fusion(bf16[1024,1,2,128]{3,0,2,1:T(8,128)(2,1)S(1)} %get-tuple-element.203, bf16[16,1024,128]{2,1,0:T(8,128)(2,1)} %get-tuple-element.202, s32[]{:T(128)} %get-tuple-element.189), kind=kOutput, calls=%fused_computation.1.clone.1 | convolution fusion | flops 541063168 | bytes 9183744 | tf_op jit(solution)/shard_map/while/body/eval_jaxpr/tkgd,rkd->tkgr/dot_general | solution.py:54
  113.5 5.5 %fusion.61 = f32[1024,1,2,128]{0,3,2,1:T(8,128)S(1)} fusion(f32[1024,1024,2]{1,0,2:T(8,128)} %get-tuple-element.178, f32[1024,2]{0,1:T(2,128)S(1)} %bitcast.127, f32[1024,1,2,128]{0,3,2,1:T(8,128)S(1)} %get-tuple-element.192, f32[1024,2]{0,1:T(2,128)S(1)} %get-tuple-element.179, pred[]{:T(512)S(6)} %compare.14, ...), kind=kOutput, calls=%fused_computation.10.clone.1 | convolution fusion | flops 543948800 | bytes 10764801 | tf_op jit(solution)/shard_map/while/body/eval_jaxpr/tkgr,rkd->tkgd/dot_general | solution.py:61
  119.4 1.4 fusion.60
  120.8 5.4 %bitcast_reduce_fusion.2 = (f32[1024,2]{0,1:T(2,128)S(1)}, f32[1024,1024,2]{1,0,2:T(8,128)}) fusion(bf16[1024,1,2,128]{3,0,2,1:T(8,128)(2,1)S(1)} %get-tuple-element.203, bf16[16,1024,128]{2,1,0:T(8,128)(2,1)} %get-tuple-element.202, s32[]{:T(128)} %get-tuple-element.189), kind=kOutput, calls=%fused_computation.1.clone.1 | convolution fusion | flops 541063168 | bytes 9183744 | tf_op jit(solution)/shard_map/while/body/eval_jaxpr/tkgd,rkd->tkgr/dot_general | solution.py:54
  126.2 5.6 %fusion.61 = f32[1024,1,2,128]{0,3,2,1:T(8,128)S(1)} fusion(f32[1024,1024,2]{1,0,2:T(8,128)} %get-tuple-element.178, f32[1024,2]{0,1:T(2,128)S(1)} %bitcast.127, f32[1024,1,2,128]{0,3,2,1:T(8,128)S(1)} %get-tuple-element.192, f32[1024,2]{0,1:T(2,128)S(1)} %get-tuple-element.179, pred[]{:T(512)S(6)} %compare.14, ...), kind=kOutput, calls=%fused_computation.10.clone.1 | convolution fusion | flops 543948800 | bytes 10764801 | tf_op jit(solution)/shard_map/while/body/eval_jaxpr/tkgr,rkd->tkgd/dot_general | solution.py:61
  132.3 1.4 fusion.60
  133.8 5.4 %bitcast_reduce_fusion.2 = (f32[1024,2]{0,1:T(2,128)S(1)}, f32[1024,1024,2]{1,0,2:T(8,128)}) fusion(bf16[1024,1,2,128]{3,0,2,1:T(8,128)(2,1)S(1)} %get-tuple-element.203, bf16[16,1024,128]{2,1,0:T(8,128)(2,1)} %get-tuple-element.202, s32[]{:T(128)} %get-tuple-element.189), kind=kOutput, calls=%fused_computation.1.clone.1 | convolution fusion | flops 541063168 | bytes 9183744 | tf_op jit(solution)/shard_map/while/body/eval_jaxpr/tkgd,rkd->tkgr/dot_general | solution.py:54
  139.2 5.5 %fusion.61 = f32[1024,1,2,128]{0,3,2,1:T(8,128)S(1)} fusion(f32[1024,1024,2]{1,0,2:T(8,128)} %get-tuple-element.178, f32[1024,2]{0,1:T(2,128)S(1)} %bitcast.127, f32[1024,1,2,128]{0,3,2,1:T(8,128)S(1)} %get-tuple-element.192, f32[1024,2]{0,1:T(2,128)S(1)} %get-tuple-element.179, pred[]{:T(512)S(6)} %compare.14, ...), kind=kOutput, calls=%fused_computation.10.clone.1 | convolution fusion | flops 543948800 | bytes 10764801 | tf_op jit(solution)/shard_map/while/body/eval_jaxpr/tkgr,rkd->tkgd/dot_general | solution.py:61
  145.1 1.4 fusion.60
  146.5 5.4 %bitcast_reduce_fusion.2 = (f32[1024,2]{0,1:T(2,128)S(1)}, f32[1024,1024,2]{1,0,2:T(8,128)}) fusion(bf16[1024,1,2,128]{3,0,2,1:T(8,128)(2,1)S(1)} %get-tuple-element.203, bf16[16,1024,128]{2,1,0:T(8,128)(2,1)} %get-tuple-element.202, s32[]{:T(128)} %get-tuple-element.189), kind=kOutput, calls=%fused_computation.1.clone.1 | convolution fusion | flops 541063168 | bytes 9183744 | tf_op jit(solution)/shard_map/while/body/eval_jaxpr/tkgd,rkd->tkgr/dot_general | solution.py:54
  152.0 5.7 %fusion.61 = f32[1024,1,2,128]{0,3,2,1:T(8,128)S(1)} fusion(f32[1024,1024,2]{1,0,2:T(8,128)} %get-tuple-element.178, f32[1024,2]{0,1:T(2,128)S(1)} %bitcast.127, f32[1024,1,2,128]{0,3,2,1:T(8,128)S(1)} %get-tuple-element.192, f32[1024,2]{0,1:T(2,128)S(1)} %get-tuple-element.179, pred[]{:T(512)S(6)} %compare.14, ...), kind=kOutput, calls=%fused_computation.10.clone.1 | convolution fusion | flops 543948800 | bytes 10764801 | tf_op jit(solution)/shard_map/while/body/eval_jaxpr/tkgr,rkd->tkgd/dot_general | solution.py:61
  158.1 1.4 fusion.60
  159.5 5.4 %bitcast_reduce_fusion.2 = (f32[1024,2]{0,1:T(2,128)S(1)}, f32[1024,1024,2]{1,0,2:T(8,128)}) fusion(bf16[1024,1,2,128]{3,0,2,1:T(8,128)(2,1)S(1)} %get-tuple-element.203, bf16[16,1024,128]{2,1,0:T(8,128)(2,1)} %get-tuple-element.202, s32[]{:T(128)} %get-tuple-element.189), kind=kOutput, calls=%fused_computation.1.clone.1 | convolution fusion | flops 541063168 | bytes 9183744 | tf_op jit(solution)/shard_map/while/body/eval_jaxpr/tkgd,rkd->tkgr/dot_general | solution.py:54
  165.0 5.5 %fusion.61 = f32[1024,1,2,128]{0,3,2,1:T(8,128)S(1)} fusion(f32[1024,1024,2]{1,0,2:T(8,128)} %get-tuple-element.178, f32[1024,2]{0,1:T(2,128)S(1)} %bitcast.127, f32[1024,1,2,128]{0,3,2,1:T(8,128)S(1)} %get-tuple-element.192, f32[1024,2]{0,1:T(2,128)S(1)} %get-tuple-element.179, pred[]{:T(512)S(6)} %compare.14, ...), kind=kOutput, calls=%fused_computation.10.clone.1 | convolution fusion | flops 543948800 | bytes 10764801 | tf_op jit(solution)/shard_map/while/body/eval_jaxpr/tkgr,rkd->tkgd/dot_general | solution.py:61
  170.9 1.4 fusion.60
  172.3 5.4 %bitcast_reduce_fusion.2 = (f32[1024,2]{0,1:T(2,128)S(1)}, f32[1024,1024,2]{1,0,2:T(8,128)}) fusion(bf16[1024,1,2,128]{3,0,2,1:T(8,128)(2,1)S(1)} %get-tuple-element.203, bf16[16,1024,128]{2,1,0:T(8,128)(2,1)} %get-tuple-element.202, s32[]{:T(128)} %get-tuple-element.189), kind=kOutput, calls=%fused_computation.1.clone.1 | convolution fusion | flops 541063168 | bytes 9183744 | tf_op jit(solution)/shard_map/while/body/eval_jaxpr/tkgd,rkd->tkgr/dot_general | solution.py:54
  177.8 5.5 %fusion.61 = f32[1024,1,2,128]{0,3,2,1:T(8,128)S(1)} fusion(f32[1024,1024,2]{1,0,2:T(8,128)} %get-tuple-element.178, f32[1024,2]{0,1:T(2,128)S(1)} %bitcast.127, f32[1024,1,2,128]{0,3,2,1:T(8,128)S(1)} %get-tuple-element.192, f32[1024,2]{0,1:T(2,128)S(1)} %get-tuple-element.179, pred[]{:T(512)S(6)} %compare.14, ...), kind=kOutput, calls=%fused_computation.10.clone.1 | convolution fusion | flops 543948800 | bytes 10764801 | tf_op jit(solution)/shard_map/while/body/eval_jaxpr/tkgr,rkd->tkgd/dot_general | solution.py:61
  183.7 1.4 fusion.60
  185.1 5.4 %bitcast_reduce_fusion.2 = (f32[1024,2]{0,1:T(2,128)S(1)}, f32[1024,1024,2]{1,0,2:T(8,128)}) fusion(bf16[1024,1,2,128]{3,0,2,1:T(8,128)(2,1)S(1)} %get-tuple-element.203, bf16[16,1024,128]{2,1,0:T(8,128)(2,1)} %get-tuple-element.202, s32[]{:T(128)} %get-tuple-element.189), kind=kOutput, calls=%fused_computation.1.clone.1 | convolution fusion | flops 541063168 | bytes 9183744 | tf_op jit(solution)/shard_map/while/body/eval_jaxpr/tkgd,rkd->tkgr/dot_general | solution.py:54
  190.5 5.5 %fusion.61 = f32[1024,1,2,128]{0,3,2,1:T(8,128)S(1)} fusion(f32[1024,1024,2]{1,0,2:T(8,128)} %get-tuple-element.178, f32[1024,2]{0,1:T(2,128)S(1)} %bitcast.127, f32[1024,1,2,128]{0,3,2,1:T(8,128)S(1)} %get-tuple-element.192, f32[1024,2]{0,1:T(2,128)S(1)} %get-tuple-element.179, pred[]{:T(512)S(6)} %compare.14, ...), kind=kOutput, calls=%fused_computation.10.clone.1 | convolution fusion | flops 543948800 | bytes 10764801 | tf_op jit(solution)/shard_map/while/body/eval_jaxpr/tkgr,rkd->tkgd/dot_general | solution.py:61
  196.6 1.4 fusion.60
  198.0 5.4 %bitcast_reduce_fusion.2 = (f32[1024,2]{0,1:T(2,128)S(1)}, f32[1024,1024,2]{1,0,2:T(8,128)}) fusion(bf16[1024,1,2,128]{3,0,2,1:T(8,128)(2,1)S(1)} %get-tuple-element.203, bf16[16,1024,128]{2,1,0:T(8,128)(2,1)} %get-tuple-element.202, s32[]{:T(128)} %get-tuple-element.189), kind=kOutput, calls=%fused_computation.1.clone.1 | convolution fusion | flops 541063168 | bytes 9183744 | tf_op jit(solution)/shard_map/while/body/eval_jaxpr/tkgd,rkd->tkgr/dot_general | solution.py:54
  203.5 5.5 %fusion.61 = f32[1024,1,2,128]{0,3,2,1:T(8,128)S(1)} fusion(f32[1024,1024,2]{1,0,2:T(8,128)} %get-tuple-element.178, f32[1024,2]{0,1:T(2,128)S(1)} %bitcast.127, f32[1024,1,2,128]{0,3,2,1:T(8,128)S(1)} %get-tuple-element.192, f32[1024,2]{0,1:T(2,128)S(1)} %get-tuple-element.179, pred[]{:T(512)S(6)} %compare.14, ...), kind=kOutput, calls=%fused_computation.10.clone.1 | convolution fusion | flops 543948800 | bytes 10764801 | tf_op jit(solution)/shard_map/while/body/eval_jaxpr/tkgr,rkd->tkgd/dot_general | solution.py:61
  209.3 1.4 fusion.60
  210.8 5.4 %bitcast_reduce_fusion.2 = (f32[1024,2]{0,1:T(2,128)S(1)}, f32[1024,1024,2]{1,0,2:T(8,128)}) fusion(bf16[1024,1,2,128]{3,0,2,1:T(8,128)(2,1)S(1)} %get-tuple-element.203, bf16[16,1024,128]{2,1,0:T(8,128)(2,1)} %get-tuple-element.202, s32[]{:T(128)} %get-tuple-element.189), kind=kOutput, calls=%fused_computation.1.clone.1 | convolution fusion | flops 541063168 | bytes 9183744 | tf_op jit(solution)/shard_map/while/body/eval_jaxpr/tkgd,rkd->tkgr/dot_general | solution.py:54
  216.2 5.5 %fusion.61 = f32[1024,1,2,128]{0,3,2,1:T(8,128)S(1)} fusion(f32[1024,1024,2]{1,0,2:T(8,128)} %get-tuple-element.178, f32[1024,2]{0,1:T(2,128)S(1)} %bitcast.127, f32[1024,1,2,128]{0,3,2,1:T(8,128)S(1)} %get-tuple-element.192, f32[1024,2]{0,1:T(2,128)S(1)} %get-tuple-element.179, pred[]{:T(512)S(6)} %compare.14, ...), kind=kOutput, calls=%fused_computation.10.clone.1 | convolution fusion | flops 543948800 | bytes 10764801 | tf_op jit(solution)/shard_map/while/body/eval_jaxpr/tkgr,rkd->tkgd/dot_general | solution.py:61
  222.1 1.4 fusion.60
  223.5 5.4 %bitcast_reduce_fusion.2 = (f32[1024,2]{0,1:T(2,128)S(1)}, f32[1024,1024,2]{1,0,2:T(8,128)}) fusion(bf16[1024,1,2,128]{3,0,2,1:T(8,128)(2,1)S(1)} %get-tuple-element.203, bf16[16,1024,128]{2,1,0:T(8,128)(2,1)} %get-tuple-element.202, s32[]{:T(128)} %get-tuple-element.189), kind=kOutput, calls=%fused_computation.1.clone.1 | convolution fusion | flops 541063168 | bytes 9183744 | tf_op jit(solution)/shard_map/while/body/eval_jaxpr/tkgd,rkd->tkgr/dot_general | solution.py:54
  229.0 5.5 %fusion.61 = f32[1024,1,2,128]{0,3,2,1:T(8,128)S(1)} fusion(f32[1024,1024,2]{1,0,2:T(8,128)} %get-tuple-element.178, f32[1024,2]{0,1:T(2,128)S(1)} %bitcast.127, f32[1024,1,2,128]{0,3,2,1:T(8,128)S(1)} %get-tuple-element.192, f32[1024,2]{0,1:T(2,128)S(1)} %get-tuple-element.179, pred[]{:T(512)S(6)} %compare.14, ...), kind=kOutput, calls=%fused_computation.10.clone.1 | convolution fusion | flops 543948800 | bytes 10764801 | tf_op jit(solution)/shard_map/while/body/eval_jaxpr/tkgr,rkd->tkgd/dot_general | solution.py:61
  234.8 1.4 fusion.60
  236.2 5.4 %bitcast_reduce_fusion.2 = (f32[1024,2]{0,1:T(2,128)S(1)}, f32[1024,1024,2]{1,0,2:T(8,128)}) fusion(bf16[1024,1,2,128]{3,0,2,1:T(8,128)(2,1)S(1)} %get-tuple-element.203, bf16[16,1024,128]{2,1,0:T(8,128)(2,1)} %get-tuple-element.202, s32[]{:T(128)} %get-tuple-element.189), kind=kOutput, calls=%fused_computation.1.clone.1 | convolution fusion | flops 541063168 | bytes 9183744 | tf_op jit(solution)/shard_map/while/body/eval_jaxpr/tkgd,rkd->tkgr/dot_general | solution.py:54
  241.7 5.5 %fusion.61 = f32[1024,1,2,128]{0,3,2,1:T(8,128)S(1)} fusion(f32[1024,1024,2]{1,0,2:T(8,128)} %get-tuple-element.178, f32[1024,2]{0,1:T(2,128)S(1)} %bitcast.127, f32[1024,1,2,128]{0,3,2,1:T(8,128)S(1)} %get-tuple-element.192, f32[1024,2]{0,1:T(2,128)S(1)} %get-tuple-element.179, pred[]{:T(512)S(6)} %compare.14, ...), kind=kOutput, calls=%fused_computation.10.clone.1 | convolution fusion | flops 543948800 | bytes 10764801 | tf_op jit(solution)/shard_map/while/body/eval_jaxpr/tkgr,rkd->tkgd/dot_general | solution.py:61
  247.5 1.4 fusion.60
  249.0 5.4 %bitcast_reduce_fusion.2 = (f32[1024,2]{0,1:T(2,128)S(1)}, f32[1024,1024,2]{1,0,2:T(8,128)}) fusion(bf16[1024,1,2,128]{3,0,2,1:T(8,128)(2,1)S(1)} %get-tuple-element.203, bf16[16,1024,128]{2,1,0:T(8,128)(2,1)} %get-tuple-element.202, s32[]{:T(128)} %get-tuple-element.189), kind=kOutput, calls=%fused_computation.1.clone.1 | convolution fusion | flops 541063168 | bytes 9183744 | tf_op jit(solution)/shard_map/while/body/eval_jaxpr/tkgd,rkd->tkgr/dot_general | solution.py:54
  254.4 5.5 %fusion.61 = f32[1024,1,2,128]{0,3,2,1:T(8,128)S(1)} fusion(f32[1024,1024,2]{1,0,2:T(8,128)} %get-tuple-element.178, f32[1024,2]{0,1:T(2,128)S(1)} %bitcast.127, f32[1024,1,2,128]{0,3,2,1:T(8,128)S(1)} %get-tuple-element.192, f32[1024,2]{0,1:T(2,128)S(1)} %get-tuple-element.179, pred[]{:T(512)S(6)} %compare.14, ...), kind=kOutput, calls=%fused_computation.10.clone.1 | convolution fusion | flops 543948800 | bytes 10764801 | tf_op jit(solution)/shard_map/while/body/eval_jaxpr/tkgr,rkd->tkgd/dot_general | solution.py:61
  260.3 1.4 fusion.60
  261.7 5.4 %bitcast_reduce_fusion.2 = (f32[1024,2]{0,1:T(2,128)S(1)}, f32[1024,1024,2]{1,0,2:T(8,128)}) fusion(bf16[1024,1,2,128]{3,0,2,1:T(8,128)(2,1)S(1)} %get-tuple-element.203, bf16[16,1024,128]{2,1,0:T(8,128)(2,1)} %get-tuple-element.202, s32[]{:T(128)} %get-tuple-element.189), kind=kOutput, calls=%fused_computation.1.clone.1 | convolution fusion | flops 541063168 | bytes 9183744 | tf_op jit(solution)/shard_map/while/body/eval_jaxpr/tkgd,rkd->tkgr/dot_general | solution.py:54
  267.2 5.5 %fusion.61 = f32[1024,1,2,128]{0,3,2,1:T(8,128)S(1)} fusion(f32[1024,1024,2]{1,0,2:T(8,128)} %get-tuple-element.178, f32[1024,2]{0,1:T(2,128)S(1)} %bitcast.127, f32[1024,1,2,128]{0,3,2,1:T(8,128)S(1)} %get-tuple-element.192, f32[1024,2]{0,1:T(2,128)S(1)} %get-tuple-element.179, pred[]{:T(512)S(6)} %compare.14, ...), kind=kOutput, calls=%fused_computation.10.clone.1 | convolution fusion | flops 543948800 | bytes 10764801 | tf_op jit(solution)/shard_map/while/body/eval_jaxpr/tkgr,rkd->tkgd/dot_general | solution.py:61
  273.0 1.4 fusion.60
  274.4 5.4 %bitcast_reduce_fusion.2 = (f32[1024,2]{0,1:T(2,128)S(1)}, f32[1024,1024,2]{1,0,2:T(8,128)}) fusion(bf16[1024,1,2,128]{3,0,2,1:T(8,128)(2,1)S(1)} %get-tuple-element.203, bf16[16,1024,128]{2,1,0:T(8,128)(2,1)} %get-tuple-element.202, s32[]{:T(128)} %get-tuple-element.189), kind=kOutput, calls=%fused_computation.1.clone.1 | convolution fusion | flops 541063168 | bytes 9183744 | tf_op jit(solution)/shard_map/while/body/eval_jaxpr/tkgd,rkd->tkgr/dot_general | solution.py:54
  279.9 5.5 %fusion.61 = f32[1024,1,2,128]{0,3,2,1:T(8,128)S(1)} fusion(f32[1024,1024,2]{1,0,2:T(8,128)} %get-tuple-element.178, f32[1024,2]{0,1:T(2,128)S(1)} %bitcast.127, f32[1024,1,2,128]{0,3,2,1:T(8,128)S(1)} %get-tuple-element.192, f32[1024,2]{0,1:T(2,128)S(1)} %get-tuple-element.179, pred[]{:T(512)S(6)} %compare.14, ...), kind=kOutput, calls=%fused_computation.10.clone.1 | convolution fusion | flops 543948800 | bytes 10764801 | tf_op jit(solution)/shard_map/while/body/eval_jaxpr/tkgr,rkd->tkgd/dot_general | solution.py:61
  285.7 1.4 fusion.60
  287.2 5.4 %bitcast_reduce_fusion.2 = (f32[1024,2]{0,1:T(2,128)S(1)}, f32[1024,1024,2]{1,0,2:T(8,128)}) fusion(bf16[1024,1,2,128]{3,0,2,1:T(8,128)(2,1)S(1)} %get-tuple-element.203, bf16[16,1024,128]{2,1,0:T(8,128)(2,1)} %get-tuple-element.202, s32[]{:T(128)} %get-tuple-element.189), kind=kOutput, calls=%fused_computation.1.clone.1 | convolution fusion | flops 541063168 | bytes 9183744 | tf_op jit(solution)/shard_map/while/body/eval_jaxpr/tkgd,rkd->tkgr/dot_general | solution.py:54
  292.6 5.5 %fusion.61 = f32[1024,1,2,128]{0,3,2,1:T(8,128)S(1)} fusion(f32[1024,1024,2]{1,0,2:T(8,128)} %get-tuple-element.178, f32[1024,2]{0,1:T(2,128)S(1)} %bitcast.127, f32[1024,1,2,128]{0,3,2,1:T(8,128)S(1)} %get-tuple-element.192, f32[1024,2]{0,1:T(2,128)S(1)} %get-tuple-element.179, pred[]{:T(512)S(6)} %compare.14, ...), kind=kOutput, calls=%fused_computation.10.clone.1 | convolution fusion | flops 543948800 | bytes 10764801 | tf_op jit(solution)/shard_map/while/body/eval_jaxpr/tkgr,rkd->tkgd/dot_general | solution.py:61
  298.5 1.4 fusion.60
  300.2 14.4 %all_to_all.24 = bf16[8,128,256]{1,2,0:T(8,128)(2,1)S(1)} all-to-all(bf16[8,128,256]{1,2,0:T(8,128)(2,1)S(1)} %copy.31), channel_id=1, replica_groups=mesh['sp'=16,'tp'=8] {'tp'}, dimensions={0} | all-to-all | bytes 1048576 | tf_op jit(solution)/shard_map/all_to_all | solution.py:107
  314.6 4.8 %multiply_reduce_fusion = (f32[128]{0:T(128)S(1)}, f32[128,2048]{1,0:T(8,128)S(1)}) fusion(bf16[128,2048]{0,1:T(8,128)(2,1)S(1)} %bitcast.129, bf16[2048,2048]{1,0:T(8,128)(2,1)} %param.18, bf16[128,2048]{1,0:T(8,128)(2,1)S(1)} %copy-done.2), kind=kOutput, calls=%fused_computation.38 | convolution fusion | flops 1074790272 | bytes 10486272 | tf_op jit(solution)/shard_map/dot_general | solution.py:108
  319.6 2.5 stack.2
  322.1 4.5 %all-to-all-start.1 = ((bf16[8,128,2048]{2,1,0:T(8,128)(2,1)}), bf16[8,128,2048]{2,1,0:T(8,128)(2,1)}, u32[]{:S(2)}, u32[]{:S(2)}) async-start(bf16[8,128,2048]{2,1,0:T(8,128)(2,1)} %stack.2), calls=%async_computation.1 | async-start | bytes 8388608 | tf_op jit(solution)/shard_map/all_to_all | solution.py:115
  326.9 49.4 %all-to-all-done.1 = bf16[8,128,2048]{2,1,0:T(8,128)(2,1)} async-done(((bf16[8,128,2048]{2,1,0:T(8,128)(2,1)}), bf16[8,128,2048]{2,1,0:T(8,128)(2,1)}, u32[]{:S(2)}, u32[]{:S(2)}) %all-to-all-start.1) | async-done | bytes 4194336 | tf_op jit(solution)/shard_map/all_to_all | solution.py:115
  376.3 14.4 %convolution_convert_fusion = bf16[1024,2048]{1,0:T(8,128)(2,1)} fusion(bf16[1024,2048]{1,0:T(8,128)(2,1)} %all-gather.8.cloned.1.call-done, bf16[1024,2048]{1,0:T(8,128)(2,1)} %bitcast.16, bf16[2048,1024]{1,0:T(8,128)(2,1)} %all-gather.6.cloned.1.call-done), kind=kOutput, calls=%fused_computation.28 | convolution fusion | flops 8595177472 | bytes 16777216 | tf_op jit(solution)/shard_map/dot_general | solution.py:127
  390.7 36.3 %reduce-scatter.2.cloned.1.call-done = bf16[128,2048]{1,0:T(8,128)(2,1)} async-done(((bf16[1024,2048]{1,0:T(8,128)(2,1)}), bf16[128,2048]{1,0:T(8,128)(2,1)}) %reduce-scatter.2.cloned.1.call-update) | async-done | bytes 524304 | tf_op jit(solution)/shard_map/reduce_scatter | solution.py:126
  427.0 1.9 add_convert_fusion
  (125 shorter events, 13.8 us)
Async XLA Ops:
  6.5 4.4 %copy-start.1 = (bf16[1024,128]{1,0:T(8,128)(2,1)S(1)}, bf16[1024,128]{1,0:T(8,128)(2,1)}, u32[]{:S(2)}) copy-start(bf16[1024,128]{1,0:T(8,128)(2,1)} %param.14) | copy-start | bytes 786436
  6.5 4.4 %copy-start.5 = (f32[128]{0:T(128)S(1)}, f32[128]{0:T(128)}, u32[]{:S(2)}) copy-start(f32[128]{0:T(128)} %param.17) | copy-start | bytes 1540
  6.5 82.9 %all-gather.4.cloned.1.call-start = ((), (), s32[]{:S(2)}) async-start(), calls=%async_computation.3 | async-start | bytes 8912896 | tf_op jit(solution)/shard_map/all_gather | solution.py:14
  8.9 6.1 %copy-start.3 = (bf16[1024,128]{1,0:T(8,128)(2,1)S(1)}, bf16[1024,128]{1,0:T(8,128)(2,1)}, u32[]{:S(2)}) copy-start(bf16[1024,128]{1,0:T(8,128)(2,1)} %param.15) | copy-start | bytes 786436
  10.9 8.1 %copy-start.6 = (f32[128]{0:T(128)S(1)}, f32[128]{0:T(128)}, u32[]{:S(2)}) copy-start(f32[128]{0:T(128)} %param.16) | copy-start | bytes 1540
  15.9 311.0 %all-gather.6.cloned.1.call-start = ((), (), s32[]{:S(2)}) async-start(), calls=%async_computation.4 | async-start | bytes 4456448 | tf_op jit(solution)/shard_map/all_gather | solution.py:120
  16.6 310.3 %all-gather.8.cloned.1.call-start = ((), (), s32[]{:S(2)}) async-start(), calls=%async_computation.5 | async-start | bytes 4456448 | tf_op jit(solution)/shard_map/all_gather | solution.py:125
  100.6 6.0 %copy-start = (f32[1024,1024,2]{1,0,2:T(8,128)S(1)}, f32[1024,1024,2]{1,0,2:T(8,128)}, u32[]{:S(2)}) copy-start(f32[1024,1024,2]{1,0,2:T(8,128)} %get-tuple-element.178) | copy-start | bytes 25165828 | tf_op jit(solution)/shard_map/while
  113.5 5.8 %copy-start = (f32[1024,1024,2]{1,0,2:T(8,128)S(1)}, f32[1024,1024,2]{1,0,2:T(8,128)}, u32[]{:S(2)}) copy-start(f32[1024,1024,2]{1,0,2:T(8,128)} %get-tuple-element.178) | copy-start | bytes 25165828 | tf_op jit(solution)/shard_map/while
  126.2 6.1 %copy-start = (f32[1024,1024,2]{1,0,2:T(8,128)S(1)}, f32[1024,1024,2]{1,0,2:T(8,128)}, u32[]{:S(2)}) copy-start(f32[1024,1024,2]{1,0,2:T(8,128)} %get-tuple-element.178) | copy-start | bytes 25165828 | tf_op jit(solution)/shard_map/while
  139.2 5.8 %copy-start = (f32[1024,1024,2]{1,0,2:T(8,128)S(1)}, f32[1024,1024,2]{1,0,2:T(8,128)}, u32[]{:S(2)}) copy-start(f32[1024,1024,2]{1,0,2:T(8,128)} %get-tuple-element.178) | copy-start | bytes 25165828 | tf_op jit(solution)/shard_map/while
  152.0 6.1 %copy-start = (f32[1024,1024,2]{1,0,2:T(8,128)S(1)}, f32[1024,1024,2]{1,0,2:T(8,128)}, u32[]{:S(2)}) copy-start(f32[1024,1024,2]{1,0,2:T(8,128)} %get-tuple-element.178) | copy-start | bytes 25165828 | tf_op jit(solution)/shard_map/while
  165.0 5.9 %copy-start = (f32[1024,1024,2]{1,0,2:T(8,128)S(1)}, f32[1024,1024,2]{1,0,2:T(8,128)}, u32[]{:S(2)}) copy-start(f32[1024,1024,2]{1,0,2:T(8,128)} %get-tuple-element.178) | copy-start | bytes 25165828 | tf_op jit(solution)/shard_map/while
  177.7 5.9 %copy-start = (f32[1024,1024,2]{1,0,2:T(8,128)S(1)}, f32[1024,1024,2]{1,0,2:T(8,128)}, u32[]{:S(2)}) copy-start(f32[1024,1024,2]{1,0,2:T(8,128)} %get-tuple-element.178) | copy-start | bytes 25165828 | tf_op jit(solution)/shard_map/while
  190.5 6.1 %copy-start = (f32[1024,1024,2]{1,0,2:T(8,128)S(1)}, f32[1024,1024,2]{1,0,2:T(8,128)}, u32[]{:S(2)}) copy-start(f32[1024,1024,2]{1,0,2:T(8,128)} %get-tuple-element.178) | copy-start | bytes 25165828 | tf_op jit(solution)/shard_map/while
  203.5 5.8 %copy-start = (f32[1024,1024,2]{1,0,2:T(8,128)S(1)}, f32[1024,1024,2]{1,0,2:T(8,128)}, u32[]{:S(2)}) copy-start(f32[1024,1024,2]{1,0,2:T(8,128)} %get-tuple-element.178) | copy-start | bytes 25165828 | tf_op jit(solution)/shard_map/while
  216.2 5.8 %copy-start = (f32[1024,1024,2]{1,0,2:T(8,128)S(1)}, f32[1024,1024,2]{1,0,2:T(8,128)}, u32[]{:S(2)}) copy-start(f32[1024,1024,2]{1,0,2:T(8,128)} %get-tuple-element.178) | copy-start | bytes 25165828 | tf_op jit(solution)/shard_map/while
  229.0 5.8 %copy-start = (f32[1024,1024,2]{1,0,2:T(8,128)S(1)}, f32[1024,1024,2]{1,0,2:T(8,128)}, u32[]{:S(2)}) copy-start(f32[1024,1024,2]{1,0,2:T(8,128)} %get-tuple-element.178) | copy-start | bytes 25165828 | tf_op jit(solution)/shard_map/while
  241.7 5.8 %copy-start = (f32[1024,1024,2]{1,0,2:T(8,128)S(1)}, f32[1024,1024,2]{1,0,2:T(8,128)}, u32[]{:S(2)}) copy-start(f32[1024,1024,2]{1,0,2:T(8,128)} %get-tuple-element.178) | copy-start | bytes 25165828 | tf_op jit(solution)/shard_map/while
  254.4 5.8 %copy-start = (f32[1024,1024,2]{1,0,2:T(8,128)S(1)}, f32[1024,1024,2]{1,0,2:T(8,128)}, u32[]{:S(2)}) copy-start(f32[1024,1024,2]{1,0,2:T(8,128)} %get-tuple-element.178) | copy-start | bytes 25165828 | tf_op jit(solution)/shard_map/while
  267.1 5.8 %copy-start = (f32[1024,1024,2]{1,0,2:T(8,128)S(1)}, f32[1024,1024,2]{1,0,2:T(8,128)}, u32[]{:S(2)}) copy-start(f32[1024,1024,2]{1,0,2:T(8,128)} %get-tuple-element.178) | copy-start | bytes 25165828 | tf_op jit(solution)/shard_map/while
  279.9 5.8 %copy-start = (f32[1024,1024,2]{1,0,2:T(8,128)S(1)}, f32[1024,1024,2]{1,0,2:T(8,128)}, u32[]{:S(2)}) copy-start(f32[1024,1024,2]{1,0,2:T(8,128)} %get-tuple-element.178) | copy-start | bytes 25165828 | tf_op jit(solution)/shard_map/while
  292.6 5.8 %copy-start = (f32[1024,1024,2]{1,0,2:T(8,128)S(1)}, f32[1024,1024,2]{1,0,2:T(8,128)}, u32[]{:S(2)}) copy-start(f32[1024,1024,2]{1,0,2:T(8,128)} %get-tuple-element.178) | copy-start | bytes 25165828 | tf_op jit(solution)/shard_map/while
  299.9 14.8 %copy-start.2 = (bf16[128,2048]{1,0:T(8,128)(2,1)S(1)}, bf16[128,2048]{1,0:T(8,128)(2,1)}, u32[]{:S(2)}) copy-start(bf16[128,2048]{1,0:T(8,128)(2,1)} %param.12) | copy-start | bytes 1572868
  314.6 4.8 %copy-start.4 = (f32[2048]{0:T(1024)S(1)}, f32[2048]{0:T(1024)}, u32[]{:S(2)}) copy-start(f32[2048]{0:T(1024)} %param.19) | copy-start | bytes 24580
  322.1 54.2 %all-to-all-start.1 = ((bf16[8,128,2048]{2,1,0:T(8,128)(2,1)}), bf16[8,128,2048]{2,1,0:T(8,128)(2,1)}, u32[]{:S(2)}, u32[]{:S(2)}) async-start(bf16[8,128,2048]{2,1,0:T(8,128)(2,1)} %stack.2), calls=%async_computation.1 | async-start | bytes 8388608 | tf_op jit(solution)/shard_map/all_to_all | solution.py:115
  326.6 100.3 %reduce-scatter.2.cloned.1.call-start = ((), (), s32[]{:S(2)}) async-start(), calls=%async_computation.6 | async-start | bytes 4718592 | tf_op jit(solution)/shard_map/reduce_scatter | solution.py:126
Sparse Core Ops, SparseCore 0:
  16.0 73.4 all-gather.3
  91.6 51.0 all-gather.5
  144.8 56.5 all-gather.7
  390.8 36.0 reduce-scatter.1
